TPU v7x, 32 devices: a whole 2x2x4 slice. The times are simulated.
32 devices in a mesh: rep: 2 (over x), fs: 8 (over z, y), tp: 2 (over core).
Axes of the slice: x: 2, y: 2, z: 4, core: 2. Of those that a mesh axis runs over, the one named last changes fastest.
Arguments:
- tokens: bfloat16 [2048, 2048], P(('rep', 'fs')), may hold values from -6 to 6
- attention_norm_gain: float32 [2048], replicated, may hold values from 0.1 to 1.9
- query_weight: bfloat16 [2048, 1024], P('fs', 'tp'), may hold values from -0.125 to 0.125
- key_weight: bfloat16 [2048, 1024], P('fs', 'tp'), may hold values from -0.125 to 0.125
- value_weight: bfloat16 [2048, 2048], P('fs', 'tp'), may hold values from -0.125 to 0.125
- decay_weight: bfloat16 [2048, 1024], P('fs', 'tp'), may hold values from -0.125 to 0.125
- decay_gate_bias: float32 [1024], P('tp'), may hold values from -1.5 to 5.5
- decay_spike_extra: float32 [2048, 32], P(('rep', 'fs'), 'tp'), may hold values from -0.7 to 0
- head_output_gain: float32 [64], replicated, may hold values from 0.1 to 1.9
- output_weight: bfloat16 [2048, 2048], P('fs', 'tp'), may hold values from -0.125 to 0.125
- channel_norm_gain: float32 [2048], replicated, may hold values from 0.1 to 1.9
- gate_weight: bfloat16 [2048, 3072], P('fs', 'tp'), may hold values from -0.125 to 0.125
- up_weight: bfloat16 [2048, 3072], P('fs', 'tp'), may hold values from -0.125 to 0.125
- down_weight: bfloat16 [2048, 3072], P('fs', 'tp'), may hold values from -0.109375 to 0.109375
Outputs:
- layer_out: bfloat16 [2048, 2048], P(('rep', 'fs'))
All inputs are finite; a program needn't handle non-finite values.
Results may differ from a plain program's by a relative error of at most 0.018.
Values may be sent and summed in bfloat16 or wider, within the bound.
A program may use at most 128 MiB of HBM per device.

v0:
```python
import jax
import jax.numpy as jnp
from jax import lax
from jax.sharding import PartitionSpec as P

BLOCK = 64
GATE_NORM = 16.0
NORM_EPS = 1e-06
HIGHEST = lax.Precision.HIGHEST


def rms_scale(values, scales):
    floats = values.astype(jnp.float32)
    return floats * lax.rsqrt(jnp.mean(floats * floats, axis=-1, keepdims=True) + NORM_EPS) * scales


def one_way(queries, key_rows, value_rows, decay_logarithm):
    length, number_of_heads, key_width = queries.shape
    value_width = value_rows.shape[2]
    block_count = length // BLOCK

    def blocks(tensor):
        return tensor.reshape(block_count, BLOCK, number_of_heads, tensor.shape[2]).transpose(
            0, 2, 1, 3
        )

    lower_mask = jnp.tril(jnp.ones((BLOCK, BLOCK), bool))

    def advance(carried, pieces):
        query_part, key_part, value_part, decay_part = pieces
        running = jnp.cumsum(decay_part, axis=1)
        spread = jnp.where(
            lower_mask[None, :, :, None], running[:, :, None, :] - running[:, None, :, :], -jnp.inf
        )
        scores = jnp.einsum(
            "hid,hjd,hijd->hij", query_part, key_part, jnp.exp(spread), precision=HIGHEST
        )
        block_end = running[:, -1:, :]
        result = jnp.einsum("hij,hje->hie", scores, value_part, precision=HIGHEST)
        result = result + jnp.einsum(
            "hid,hde->hie", query_part * jnp.exp(running), carried, precision=HIGHEST
        )
        carried = jnp.exp(block_end)[:, 0, :, None] * carried + jnp.einsum(
            "hjd,hje->hde", key_part * jnp.exp(block_end - running), value_part, precision=HIGHEST
        )
        return (carried, result)

    zero_state = jnp.zeros((number_of_heads, key_width, value_width), jnp.float32)
    _, outputs = lax.scan(
        advance,
        zero_state,
        (blocks(queries), blocks(key_rows), blocks(value_rows), blocks(decay_logarithm)),
    )
    return outputs.transpose(0, 2, 1, 3).reshape(length, number_of_heads, value_width)


def both_ways(queries, key_rows, value_rows, decay_logarithm):
    forward = one_way(queries, key_rows, value_rows, decay_logarithm)
    backward = one_way(
        jnp.flip(queries, 0),
        jnp.flip(key_rows, 0),
        jnp.flip(value_rows, 0),
        jnp.flip(decay_logarithm, 0),
    )
    return forward + jnp.flip(backward, 0)


def rounded(floats):
    return lax.optimization_barrier(floats.astype(jnp.bfloat16)).astype(jnp.float32)


def shards(
    tokens,
    attention_norm_gain,
    query_weight,
    key_weight,
    value_weight,
    decay_weight,
    decay_gate_bias,
    decay_spike_extra,
    head_output_gain,
    output_weight,
    channel_norm_gain,
    gate_weight,
    up_weight,
    down_weight,
):
    full_query, full_key, full_value, full_decay, full_output = (
        lax.all_gather(query_weight, "fs", axis=0, tiled=True),
        lax.all_gather(key_weight, "fs", axis=0, tiled=True),
        lax.all_gather(value_weight, "fs", axis=0, tiled=True),
        lax.all_gather(decay_weight, "fs", axis=0, tiled=True),
        lax.all_gather(output_weight, "fs", axis=0, tiled=True),
    )
    normed = rms_scale(tokens, attention_norm_gain).astype(jnp.bfloat16)
    narrow = full_query.shape[1]
    wide_cols = full_value.shape[1]
    length = normed.shape[0]
    number_of_heads = decay_spike_extra.shape[1]
    key_width = narrow // number_of_heads
    value_width = wide_cols // number_of_heads
    query_proj = jnp.dot(normed, full_query, preferred_element_type=jnp.float32)
    key_proj = jnp.dot(normed, full_key, preferred_element_type=jnp.float32)
    value_proj = jnp.dot(normed, full_value, preferred_element_type=jnp.float32)
    gate_pre = jnp.dot(normed, full_decay, preferred_element_type=jnp.float32)
    queries = (rounded(query_proj) * key_width ** (-0.5)).reshape(
        length, number_of_heads, key_width
    )
    key_rows = rounded(key_proj).reshape(length, number_of_heads, key_width)
    value_rows = rounded(value_proj).reshape(length, number_of_heads, value_width)
    decay_logarithm = (
        jax.nn.log_sigmoid(gate_pre + decay_gate_bias).reshape(length, number_of_heads, key_width)
        / GATE_NORM
    )
    decay_logarithm = decay_logarithm + decay_spike_extra[:, :, None]
    mixed_heads = both_ways(queries, key_rows, value_rows, decay_logarithm)
    attended = (
        rms_scale(mixed_heads, head_output_gain).reshape(length, wide_cols).astype(jnp.bfloat16)
    )
    full_gate, full_up, full_down = (
        lax.all_gather(gate_weight, "fs", axis=0, tiled=True),
        lax.all_gather(up_weight, "fs", axis=0, tiled=True),
        lax.all_gather(down_weight, "fs", axis=0, tiled=True),
    )
    mixer_term = lax.dot_general(
        attended, full_output, (((1,), (1,)), ((), ())), preferred_element_type=jnp.float32
    )
    mixed_sum = lax.psum(mixer_term.astype(jnp.bfloat16), "tp").astype(jnp.float32)
    residual = (tokens.astype(jnp.float32) + mixed_sum).astype(jnp.bfloat16)
    normed_two = rms_scale(residual, channel_norm_gain).astype(jnp.bfloat16)
    gate_part = jnp.dot(normed_two, full_gate, preferred_element_type=jnp.float32)
    up_part = jnp.dot(normed_two, full_up, preferred_element_type=jnp.float32)
    hidden = (jax.nn.silu(gate_part) * up_part).astype(jnp.bfloat16)
    channel_term = lax.dot_general(
        hidden, full_down, (((1,), (1,)), ((), ())), preferred_element_type=jnp.float32
    )
    channel_sum = lax.psum(channel_term.astype(jnp.bfloat16), "tp").astype(jnp.float32)
    return (residual.astype(jnp.float32) + channel_sum).astype(jnp.bfloat16)


def solution(mesh):
    in_specs = (
        P(("rep", "fs"), None),
        P(),
        P("fs", "tp"),
        P("fs", "tp"),
        P("fs", "tp"),
        P("fs", "tp"),
        P("tp"),
        P(("rep", "fs"), "tp"),
        P(),
        P("fs", "tp"),
        P(),
        P("fs", "tp"),
        P("fs", "tp"),
        P("fs", "tp"),
    )
    out_specs = P(("rep", "fs"), None)
    return jax.shard_map(shards, mesh=mesh, in_specs=in_specs, out_specs=out_specs, check_vma=False)
```

profile of v0, /device:TPU:0, one launch (start us, length us, event | category | flops | bytes accessed | tf_op | source)
XLA Modules:
  0.0 797.3 jit_solution(2030128879946733997)
XLA Ops:
  12.0 49.3 %all-gather.9.cloned.1.call-done = bf16[2048,512]{1,0:T(8,128)(2,1)} async-done(((bf16[256,512]{1,0:T(8,128)(2,1)}), bf16[2048,512]{1,0:T(8,128)(2,1)}) %all-gather.9.cloned.1.call-update) | async-done | bytes 2097168 | tf_op jit(solution)/shard_map/all_gather | solution.py:92
  61.3 2.4 fusion.48
  64.4 1.4 copy.131
  65.7 45.4 %all-gather.15.cloned.1.call-done = bf16[2048,512]{1,0:T(8,128)(2,1)} async-done(((bf16[256,512]{1,0:T(8,128)(2,1)}), bf16[2048,512]{1,0:T(8,128)(2,1)}) %all-gather.15.cloned.1.call-update) | async-done | bytes 2097168 | tf_op jit(solution)/shard_map/all_gather | solution.py:89
  111.1 2.1 convolution_convert_fusion.3
  115.1 45.8 %all-gather.11.cloned.1.call-done = bf16[2048,512]{1,0:T(8,128)(2,1)} async-done(((bf16[256,512]{1,0:T(8,128)(2,1)}), bf16[2048,512]{1,0:T(8,128)(2,1)}) %all-gather.11.cloned.1.call-update) | async-done | bytes 2097168 | tf_op jit(solution)/shard_map/all_gather | solution.py:90
  160.9 2.1 convolution_convert_fusion.4
  164.3 1.4 copy.132
  166.7 67.5 %all-gather.13.cloned.1.call-done = bf16[2048,1024]{1,0:T(8,128)(2,1)} async-done(((bf16[256,1024]{1,0:T(8,128)(2,1)}), bf16[2048,1024]{1,0:T(8,128)(2,1)}) %all-gather.13.cloned.1.call-update) | async-done | bytes 4194320 | tf_op jit(solution)/shard_map/all_gather | solution.py:91
  234.2 2.9 convolution_convert_fusion.2
  238.8 1.7 reshape.80
  241.6 90.0 %while.27 = (s32[]{:T(128)}, f32[16,32,64]{2,1,0:T(8,128)}, f32[2,16,64,64]{3,2,1,0:T(8,128)}, f32[2,16,64,32]{3,1,2,0:T(8,128)}, f32[2,16,64,32]{3,1,2,0:T(8,12...) while((s32[]{:T(128)}, f32[16,32,64]{2,1,0:T(8,128)}, ...), condition=%wide.region_6.7_spmd.clone, body=%wide.region_4.6_spmd.clone.sunk | while | flops 113446912 | bytes 41307280 | solution.py:49
  243.1 8.4 %select_exponential_fusion.5 = f32[16,64,64,32]{2,3,1,0:T(8,128)} fusion(f32[16,64,32]{1,2,0:T(8,128)S(1)} %copy.175, f32[16,64,32]{2,1,0:T(8,128)S(1)} %copy.176, pred[64,64]{1,0:T(8,128)(4,1)S(1)} %iota_compare_fusion.5), kind=kLoop, calls=%fused_computation.34.clone.1 | loop fusion | flops 4194304 | bytes 8654848 | tf_op jit(solution)/shard_map/while/body/eval_jaxpr/exp | solution.py:36
  251.5 18.5 %copy.177 = f32[16,64,64,32]{1,2,3,0:T(8,128)} copy(f32[16,64,64,32]{2,3,1,0:T(8,128)} %select_exponential_fusion.5) | data formatting | bytes 16777216 | tf_op jit(solution)/shard_map/while
  271.6 7.7 fusion.114
  280.3 1.8 constant_dynamic-slice_fusion.9
  282.1 1.8 fusion.115
  283.9 1.8 convolution_add_fusion.8
  287.2 8.4 %select_exponential_fusion.5 = f32[16,64,64,32]{2,3,1,0:T(8,128)} fusion(f32[16,64,32]{1,2,0:T(8,128)S(1)} %copy.175, f32[16,64,32]{2,1,0:T(8,128)S(1)} %copy.176, pred[64,64]{1,0:T(8,128)(4,1)S(1)} %iota_compare_fusion.5), kind=kLoop, calls=%fused_computation.34.clone.1 | loop fusion | flops 4194304 | bytes 8654848 | tf_op jit(solution)/shard_map/while/body/eval_jaxpr/exp | solution.py:36
  295.6 18.4 %copy.177 = f32[16,64,64,32]{1,2,3,0:T(8,128)} copy(f32[16,64,64,32]{2,3,1,0:T(8,128)} %select_exponential_fusion.5) | data formatting | bytes 16777216 | tf_op jit(solution)/shard_map/while
  315.6 7.7 fusion.114
  323.5 1.7 fusion.113
  325.2 1.8 constant_dynamic-slice_fusion.9
  327.0 1.8 fusion.115
  328.8 2.7 convolution_add_fusion.8
  331.5 1.6 copy.116
  334.7 2.5 copy.149
  338.4 98.9 %while.26 = (s32[]{:T(128)}, f32[16,32,64]{2,1,0:T(8,128)S(1)}, f32[2,16,64,64]{3,2,1,0:T(8,128)}, f32[2,16,64,32]{2,0,3,1:T(2,128)}, f32[2,16,64,32]{2,0,3,1:T(...) while((s32[]{:T(128)}, f32[16,32,64]{2,1,0:T(8,128)S(1)}, ...), condition=%wide.region_3.4_spmd.clone, body=%wide.region_1.3_spmd.clone.sunk | while | flops 113446912 | bytes 47736008 | solution.py:49
  340.0 6.3 fusion.101
  346.4 1.8 constant_dynamic-slice_fusion.7
  350.0 8.4 %select_exponential_fusion.4 = f32[16,64,64,32]{2,3,1,0:T(8,128)} fusion(f32[16,64,32]{1,2,0:T(8,128)S(1)} %copy.170, f32[16,64,32]{2,1,0:T(8,128)S(1)} %copy.171, pred[64,64]{1,0:T(8,128)(4,1)S(1)} %iota_compare_fusion.4), kind=kLoop, calls=%fused_computation.4.clone.1 | loop fusion | flops 4194304 | bytes 8654848 | tf_op jit(solution)/shard_map/while/body/eval_jaxpr/exp | solution.py:36
  358.4 18.4 %copy.172 = f32[16,64,64,32]{1,2,3,0:T(8,128)} copy(f32[16,64,64,32]{2,3,1,0:T(8,128)} %select_exponential_fusion.4) | data formatting | bytes 16777216 | tf_op jit(solution)/shard_map/while
  376.8 7.8 fusion.103
  389.4 6.3 fusion.101
  395.8 1.8 constant_dynamic-slice_fusion.7
  399.5 8.4 %select_exponential_fusion.4 = f32[16,64,64,32]{2,3,1,0:T(8,128)} fusion(f32[16,64,32]{1,2,0:T(8,128)S(1)} %copy.170, f32[16,64,32]{2,1,0:T(8,128)S(1)} %copy.171, pred[64,64]{1,0:T(8,128)(4,1)S(1)} %iota_compare_fusion.4), kind=kLoop, calls=%fused_computation.4.clone.1 | loop fusion | flops 4194304 | bytes 8654848 | tf_op jit(solution)/shard_map/while/body/eval_jaxpr/exp | solution.py:36
  407.9 18.4 %copy.172 = f32[16,64,64,32]{1,2,3,0:T(8,128)} copy(f32[16,64,64,32]{2,3,1,0:T(8,128)} %select_exponential_fusion.4) | data formatting | bytes 16777216 | tf_op jit(solution)/shard_map/while
  426.3 7.8 fusion.103
  437.3 1.6 copy.107
  440.8 4.5 convolution_convert_fusion.1
  447.9 14.8 %all-reduce.3.cloned.1.call-done = bf16[128,2048]{1,0:T(8,128)(2,1)} async-done(((bf16[128,2048]{1,0:T(8,128)(2,1)}), bf16[128,2048]{1,0:T(8,128)(2,1)}) %all-reduce.3.cloned.1.call-update) | async-done | bytes 524304 | tf_op jit(solution)/shard_map/psum | solution.py:128
  464.0 100.8 %all-gather.19.cloned.1.call-done = bf16[2048,1536]{1,0:T(8,128)(2,1)} async-done(((bf16[256,1536]{1,0:T(8,128)(2,1)}), bf16[2048,1536]{1,0:T(8,128)(2,1)}) %all-gather.19.cloned.1.call-update) | async-done | bytes 6291472 | tf_op jit(solution)/shard_map/all_gather | solution.py:121
  564.8 3.8 fusion.51
  568.6 95.3 %all-gather.21.cloned.1.call-done = bf16[2048,1536]{1,0:T(8,128)(2,1)} async-done(((bf16[256,1536]{1,0:T(8,128)(2,1)}), bf16[2048,1536]{1,0:T(8,128)(2,1)}) %all-gather.21.cloned.1.call-update) | async-done | bytes 6291472 | tf_op jit(solution)/shard_map/all_gather | solution.py:122
  663.9 99.1 %all-gather.23.cloned.1.call-done = bf16[2048,1536]{1,0:T(8,128)(2,1)} async-done(((bf16[256,1536]{1,0:T(8,128)(2,1)}), bf16[2048,1536]{1,0:T(8,128)(2,1)}) %all-gather.23.cloned.1.call-update) | async-done | bytes 6291472 | tf_op jit(solution)/shard_map/all_gather | solution.py:123
  763.0 8.6 %convolution_convert_fusion = bf16[128,2048]{1,0:T(8,128)(2,1)} fusion(bf16[2048,1536]{1,0:T(8,128)(2,1)} %all-gather.23.cloned.1.call-done, bf16[2048,1536]{1,0:T(8,128)(2,1)} %all-gather.21.cloned.1.call-done, f32[128,1536]{1,0:T(8,128)S(1)} %fusion.51, bf16[128,2048]{1,0:T(8,128)(2,1)S(1)} %get-tuple-element.214, f32[2048]{0:T(1024)S(1)} %copy-done.8, ...), kind=kOutput, calls=%fused_computation.60 | convolution fusion | flops 1613103104 | bytes 14426624 | tf_op jit(solution)/shard_map/dot_general | solution.py:134
  771.5 16.9 %all-reduce.5.cloned.1.call-done = bf16[128,2048]{1,0:T(8,128)(2,1)} async-done(((bf16[128,2048]{1,0:T(8,128)(2,1)}), bf16[128,2048]{1,0:T(8,128)(2,1)}) %all-reduce.5.cloned.1.call-update) | async-done | bytes 524304 | tf_op jit(solution)/shard_map/psum | solution.py:137
  788.5 2.0 fusion.45
  (123 shorter events, 42.0 us)
Async XLA Ops:
  6.5 104.5 %copy-start.2 = (bf16[128,2048]{1,0:T(8,128)(2,1)S(1)}, bf16[128,2048]{1,0:T(8,128)(2,1)}, u32[]{:S(2)}) copy-start(bf16[128,2048]{1,0:T(8,128)(2,1)} %param.18) | copy-start | bytes 1572868
  6.5 57.7 %copy-start.6 = (f32[128,16]{0,1:T(8,128)S(1)}, f32[128,16]{0,1:T(8,128)}, u32[]{:S(2)}) copy-start(f32[128,16]{0,1:T(8,128)} %param.25) | copy-start | bytes 24580
  6.5 104.5 %copy-start.7 = (f32[2048]{0:T(1024)S(1)}, f32[2048]{0:T(1024)}, u32[]{:S(2)}) copy-start(f32[2048]{0:T(1024)} %param.19) | copy-start | bytes 24580
  6.5 54.8 %all-gather.9.cloned.1.call-start = ((), (), s32[]{:S(2)}) async-start(), calls=%async_computation | async-start | bytes 2359296 | tf_op jit(solution)/shard_map/all_gather | solution.py:92
  7.3 103.8 %all-gather.15.cloned.1.call-start = ((), (), s32[]{:S(2)}) async-start(), calls=%async_computation.3 | async-start | bytes 2359296 | tf_op jit(solution)/shard_map/all_gather | solution.py:89
  8.0 152.9 %all-gather.11.cloned.1.call-start = ((), (), s32[]{:S(2)}) async-start(), calls=%async_computation.1 | async-start | bytes 2359296 | tf_op jit(solution)/shard_map/all_gather | solution.py:90
  8.7 225.5 %all-gather.13.cloned.1.call-start = ((), (), s32[]{:S(2)}) async-start(), calls=%async_computation.2 | async-start | bytes 4718592 | tf_op jit(solution)/shard_map/all_gather | solution.py:91
  9.3 431.5 %all-gather.17.cloned.1.call-start = ((), (), s32[]{:S(2)}) async-start(), calls=%async_computation.4 | async-start | bytes 4718592 | tf_op jit(solution)/shard_map/all_gather | solution.py:93
  9.9 452.7 %all-reduce.3.cloned.1.call-start = ((), (), s32[]{:S(2)}) async-start(), calls=%async_computation.5 | async-start | bytes 1048576 | tf_op jit(solution)/shard_map/psum | solution.py:128
  271.6 7.7 copy-start
  315.6 7.7 copy-start
  338.4 102.2 %copy-start.9 = (f32[64]{0:T(128)S(1)}, f32[64]{0:T(128)}, u32[]{:S(2)}) copy-start(f32[64]{0:T(128)} %param.26) | copy-start | bytes 772
  376.8 7.8 copy-start.1
  376.8 7.9 copy-start.4
  385.7 1.0 copy-start.5
  426.3 7.8 copy-start.1
  426.3 7.9 copy-start.4
  435.2 1.0 copy-start.5
  438.9 23.8 %copy-start.3 = (bf16[128,2048]{1,0:T(8,128)(2,1)S(1)}, bf16[128,2048]{1,0:T(8,128)(2,1)}, u32[]{:S(2)}) copy-start(bf16[128,2048]{1,0:T(8,128)(2,1)} %param.18) | copy-start | bytes 1572868
  439.5 125.3 %copy-start.8 = (f32[2048]{0:T(1024)S(1)}, f32[2048]{0:T(1024)}, u32[]{:S(2)}) copy-start(f32[2048]{0:T(1024)} %param.28) | copy-start | bytes 24580
  445.3 119.5 %all-gather.19.cloned.1.call-start = ((), (), s32[]{:S(2)}) async-start(), calls=%async_computation.6 | async-start | bytes 7077888 | tf_op jit(solution)/shard_map/all_gather | solution.py:121
  446.1 217.8 %all-gather.21.cloned.1.call-start = ((), (), s32[]{:S(2)}) async-start(), calls=%async_computation.7 | async-start | bytes 7077888 | tf_op jit(solution)/shard_map/all_gather | solution.py:122
  446.8 316.1 %all-gather.23.cloned.1.call-start = ((), (), s32[]{:S(2)}) async-start(), calls=%async_computation.8 | async-start | bytes 7077888 | tf_op jit(solution)/shard_map/all_gather | solution.py:123
  447.5 340.9 %all-reduce.5.cloned.1.call-start = ((), (), s32[]{:S(2)}) async-start(), calls=%async_computation.9 | async-start | bytes 1048576 | tf_op jit(solution)/shard_map/psum | solution.py:137
Sparse Core Ops, SparseCore 0:
  9.5 51.7 all-gather.8
  63.4 47.6 all-gather.14
  113.2 47.6 all-gather.10
  162.8 71.3 all-gather.12
  236.2 71.3 all-gather.16
  445.4 17.1 all-reduce.2
  464.8 99.8 all-gather.18
  566.9 96.8 all-gather.20
  666.0 96.8 all-gather.22
  771.7 16.7 all-reduce.4
where the time goes:
time: 799 us; the launch traced here: 797 us
  waiting for transfers between devices  540 us (68%)
  local copies, waits for them, and re-layouts  113 us (14%)
  other arithmetic  87 us (11%)
  matrix products  42.7 us (5%)
  between operations  13.8 us (2%)
    all_gather x1, waiting for transfers between devices, shards(): lax.all_gather(gate_weight, 'fs', axis=0, tiled=True)  101 us
    all_gather x1, waiting for transfers between devices, shards(): lax.all_gather(down_weight, 'fs', axis=0, tiled=True)  99.1 us
    all_gather x1, waiting for transfers between devices, shards(): lax.all_gather(up_weight, 'fs', axis=0, tiled=True)  95.3 us
    while x20, local copies, waits for them, and re-layouts  75.6 us
    all_gather x1, waiting for transfers between devices, shards(): lax.all_gather(value_weight, 'fs', axis=0, tiled=True)  67.5 us
    all_gather x1, waiting for transfers between devices, shards(): lax.all_gather(decay_weight, 'fs', axis=0, tiled=True)  49.3 us
    all_gather x1, waiting for transfers between devices, shards(): lax.all_gather(key_weight, 'fs', axis=0, tiled=True)  45.8 us
    all_gather x1, waiting for transfers between devices, shards(): lax.all_gather(query_weight, 'fs', axis=0, tiled=True)  45.4 us
  transfers between devices with their start and end apart: 10, of which 9 were waited for; matrix products, arithmetic and copies ran while one was open for 28% of the time, Pallas kernels for 0%

commit v1 on v0

--- a/solution.py
+++ b/solution.py
@@ -7,6 +7,24 @@
 GATE_NORM = 16.0
 NORM_EPS = 1e-06
 HIGHEST = lax.Precision.HIGHEST
+
+
+def ring_gather(array, axis, dim):
+    ways, here, turn = (lax.axis_size(axis), lax.axis_index(axis), array.shape[dim])
+    shape = [n * ways if d == dim else n for d, n in enumerate(array.shape)]
+    full = lax.dynamic_update_slice_in_dim(
+        jnp.zeros(shape, array.dtype), array, here * turn, axis=dim
+    )
+    going_up = going_down = array
+    for far in range(1, ways // 2 + 1):
+        going_up = lax.ppermute(going_up, axis, [(d, (d + 1) % ways) for d in range(ways)])
+        full = lax.dynamic_update_slice_in_dim(full, going_up, (here - far) % ways * turn, axis=dim)
+        if 2 * far < ways:
+            going_down = lax.ppermute(going_down, axis, [(d, (d - 1) % ways) for d in range(ways)])
+            full = lax.dynamic_update_slice_in_dim(
+                full, going_down, (here + far) % ways * turn, axis=dim
+            )
+    return full
 
 
 def rms_scale(values, scales):
@@ -119,7 +137,7 @@
     )
     full_gate, full_up, full_down = (
         lax.all_gather(gate_weight, "fs", axis=0, tiled=True),
-        lax.all_gather(up_weight, "fs", axis=0, tiled=True),
+        ring_gather(up_weight, "fs", 0),
         lax.all_gather(down_weight, "fs", axis=0, tiled=True),
     )
     mixer_term = lax.dot_general(

time: 799 us -> 771 us (0.965)
  waiting for transfers between devices: 540 us -> 478 us
  local copies, waits for them, and re-layouts: 113 us -> 129 us
  starting transfers between devices: 0.61 us -> 15.1 us
    ppermute x0 -> x7, waiting for transfers between devices: none -> 132 us  [the longest x4 124 us: ring_gather(): lax.ppermute(going_up, axis, [(d, (d + 1) % ways) for d in range(ways)])]
    all_gather x1 -> x0, waiting for transfers between devices: 95.3 us -> none  [shards(): lax.all_gather(up_weight, 'fs', axis=0, tiled=True)]
    all_gather x1, waiting for transfers between devices: 101 us -> 20.4 us  [shards(): lax.all_gather(gate_weight, 'fs', axis=0, tiled=True)]
    ppermute x0 -> x7, starting transfers between devices: none -> 14.8 us  [the longest x4 7.67 us: ring_gather(): lax.ppermute(going_up, axis, [(d, (d + 1) % ways) for d in range(ways)])]
    psum x1, waiting for transfers between devices: 14.8 us -> 0.01 us  [shards(): lax.psum(mixer_term.astype(jnp.bfloat16), 'tp').astype(jnp.float32)]
    dynamic_update_slice x0 -> x8, local copies, waits for them, and re-layouts: none -> 11 us  [the longest x3 5.08 us: ring_gather(): lax.dynamic_update_slice_in_dim(full, going_down, (here + far) % ways * t...]
    while x20 -> x32, local copies, waits for them, and re-layouts: 75.6 us -> 77.5 us
  transfers between devices with their start and end apart: 10 -> 16, of which waited for: 9 -> 13; matrix products, arithmetic and copies ran while one was open for 28% -> 32% of each run, Pallas kernels for 0% -> 0%
where the time goes in v1:
time: 771 us; the launch traced here: 769 us
  waiting for transfers between devices  478 us (62%)
  local copies, waits for them, and re-layouts  129 us (17%)
  other arithmetic  90.1 us (12%)
  matrix products  43.2 us (6%)
  starting transfers between devices  15.1 us (2%)
  between operations  13.5 us (2%)
    ppermute x4, waiting for transfers between devices, ring_gather(): lax.ppermute(going_up, axis, [(d, (d + 1) % ways) for d in range(ways)])  124 us
    all_gather x1, waiting for transfers between devices, shards(): lax.all_gather(down_weight, 'fs', axis=0, tiled=True)  95.9 us
    while x32, local copies, waits for them, and re-layouts  77.5 us
    all_gather x1, waiting for transfers between devices, shards(): lax.all_gather(value_weight, 'fs', axis=0, tiled=True)  64.4 us
    all_gather x1, waiting for transfers between devices, shards(): lax.all_gather(decay_weight, 'fs', axis=0, tiled=True)  49.3 us
    all_gather x1, waiting for transfers between devices, shards(): lax.all_gather(query_weight, 'fs', axis=0, tiled=True)  47.3 us
    all_gather x1, waiting for transfers between devices, shards(): lax.all_gather(key_weight, 'fs', axis=0, tiled=True)  46.9 us
    exp x4, other arithmetic, advance(): jnp.exp(spread)  34.2 us
  transfers between devices with their start and end apart: 16, of which 13 were waited for; matrix products, arithmetic and copies ran while one was open for 32% of the time, Pallas kernels for 0%

profile of v1, /device:TPU:0, one launch (start us, length us, event | category | flops | bytes accessed | tf_op | source)
XLA Modules:
  0.0 768.8 jit_solution(8184539226253125712)
XLA Ops:
  12.0 49.3 %all-gather.8.cloned.1.call-done = bf16[2048,512]{1,0:T(8,128)(2,1)} async-done(((bf16[256,512]{1,0:T(8,128)(2,1)}), bf16[2048,512]{1,0:T(8,128)(2,1)}) %all-gather.8.cloned.1.call-update) | async-done | bytes 2097168 | tf_op jit(solution)/shard_map/all_gather | solution.py:110
  61.3 2.4 fusion.48
  64.2 46.9 %all-gather.10.cloned.1.call-done = bf16[2048,512]{1,0:T(8,128)(2,1)} async-done(((bf16[256,512]{1,0:T(8,128)(2,1)}), bf16[2048,512]{1,0:T(8,128)(2,1)}) %all-gather.10.cloned.1.call-update) | async-done | bytes 2097168 | tf_op jit(solution)/shard_map/all_gather | solution.py:108
  111.1 2.1 convolution_convert_fusion.4
  113.6 47.3 %all-gather.14.cloned.1.call-done = bf16[2048,512]{1,0:T(8,128)(2,1)} async-done(((bf16[256,512]{1,0:T(8,128)(2,1)}), bf16[2048,512]{1,0:T(8,128)(2,1)}) %all-gather.14.cloned.1.call-update) | async-done | bytes 2097168 | tf_op jit(solution)/shard_map/all_gather | solution.py:107
  160.9 2.1 convolution_convert_fusion.3
  169.8 64.4 %all-gather.12.cloned.1.call-done = bf16[2048,1024]{1,0:T(8,128)(2,1)} async-done(((bf16[256,1024]{1,0:T(8,128)(2,1)}), bf16[2048,1024]{1,0:T(8,128)(2,1)}) %all-gather.12.cloned.1.call-update) | async-done | bytes 4194320 | tf_op jit(solution)/shard_map/all_gather | solution.py:109
  234.2 2.9 convolution_convert_fusion.2
  240.8 101.7 %while.26 = (s32[]{:T(128)}, f32[16,32,64]{2,1,0:T(8,128)S(1)}, f32[2,16,64,64]{3,2,1,0:T(8,128)}, f32[2,16,64,32]{2,0,3,1:T(2,128)}, f32[2,16,64,32]{2,0,3,1:T(...) while((s32[]{:T(128)}, f32[16,32,64]{2,1,0:T(8,128)S(1)}, ...), condition=%wide.region_3.4_spmd.clone, body=%wide.region_1.3_spmd.clone.sunk | while | flops 113446912 | bytes 49302792 | solution.py:67
  244.6 6.3 fusion.101
  252.1 2.1 convolution_add_fusion.7
  254.7 8.6 %select_exponential_fusion.4 = f32[16,64,64,32]{2,3,1,0:T(8,128)} fusion(f32[16,64,32]{1,2,0:T(8,128)S(1)} %copy.170, f32[16,64,32]{2,1,0:T(8,128)S(1)} %copy.171, pred[64,64]{1,0:T(8,128)(4,1)S(1)} %iota_compare_fusion.4), kind=kLoop, calls=%fused_computation.4.clone.1 | loop fusion | flops 4194304 | bytes 8654848 | tf_op jit(solution)/shard_map/while/body/eval_jaxpr/exp | solution.py:54
  263.3 18.4 %copy.172 = f32[16,64,64,32]{1,2,3,0:T(8,128)} copy(f32[16,64,64,32]{2,3,1,0:T(8,128)} %select_exponential_fusion.4) | data formatting | bytes 16777216 | tf_op jit(solution)/shard_map/while
  281.7 8.0 %fusion.103 = f32[16,64,64]{1,2,0:T(8,128)S(1)} fusion(f32[16,64,64,32]{1,2,3,0:T(8,128)} %copy.172, f32[16,32,64]{2,1,0:T(8,128)S(1)} %bitcast.159, f32[16,32,64]{2,1,0:T(8,128)S(1)} %bitcast.160), kind=kLoop, calls=%fused_computation.3.clone.1 | loop fusion | flops 6225920 | bytes 8912896 | tf_op jit(solution)/shard_map/while/body/eval_jaxpr/hid,hjd,hijd->hij/dot_general | solution.py:53
  295.5 6.3 fusion.101
  303.0 2.1 convolution_add_fusion.7
  305.6 8.6 %select_exponential_fusion.4 = f32[16,64,64,32]{2,3,1,0:T(8,128)} fusion(f32[16,64,32]{1,2,0:T(8,128)S(1)} %copy.170, f32[16,64,32]{2,1,0:T(8,128)S(1)} %copy.171, pred[64,64]{1,0:T(8,128)(4,1)S(1)} %iota_compare_fusion.4), kind=kLoop, calls=%fused_computation.4.clone.1 | loop fusion | flops 4194304 | bytes 8654848 | tf_op jit(solution)/shard_map/while/body/eval_jaxpr/exp | solution.py:54
  314.2 18.4 %copy.172 = f32[16,64,64,32]{1,2,3,0:T(8,128)} copy(f32[16,64,64,32]{2,3,1,0:T(8,128)} %select_exponential_fusion.4) | data formatting | bytes 16777216 | tf_op jit(solution)/shard_map/while
  332.5 8.0 %fusion.103 = f32[16,64,64]{1,2,0:T(8,128)S(1)} fusion(f32[16,64,64,32]{1,2,3,0:T(8,128)} %copy.172, f32[16,32,64]{2,1,0:T(8,128)S(1)} %bitcast.159, f32[16,32,64]{2,1,0:T(8,128)S(1)} %bitcast.160), kind=kLoop, calls=%fused_computation.3.clone.1 | loop fusion | flops 6225920 | bytes 8912896 | tf_op jit(solution)/shard_map/while/body/eval_jaxpr/hid,hjd,hijd->hij/dot_general | solution.py:53
  349.6 92.6 %while.27 = (s32[]{:T(128)}, f32[16,32,64]{2,1,0:T(8,128)}, f32[2,16,64,64]{3,2,1,0:T(8,128)}, f32[2,16,64,32]{3,1,2,0:T(8,128)}, f32[2,16,64,32]{3,1,2,0:T(8,12...) while((s32[]{:T(128)}, f32[16,32,64]{2,1,0:T(8,128)}, ...), condition=%wide.region_6.7_spmd.clone, body=%wide.region_4.6_spmd.clone.sunk | while | flops 113446912 | bytes 45238460 | solution.py:67
  356.7 8.6 %select_exponential_fusion.5 = f32[16,64,64,32]{2,3,1,0:T(8,128)} fusion(f32[16,64,32]{1,2,0:T(8,128)S(1)} %copy.175, f32[16,64,32]{2,1,0:T(8,128)S(1)} %copy.176, pred[64,64]{1,0:T(8,128)(4,1)S(1)} %iota_compare_fusion.5), kind=kLoop, calls=%fused_computation.34.clone.1 | loop fusion | flops 4194304 | bytes 8654848 | tf_op jit(solution)/shard_map/while/body/eval_jaxpr/exp | solution.py:54
  365.3 18.4 %copy.177 = f32[16,64,64,32]{1,2,3,0:T(8,128)} copy(f32[16,64,64,32]{2,3,1,0:T(8,128)} %select_exponential_fusion.5) | data formatting | bytes 16777216 | tf_op jit(solution)/shard_map/while
  385.3 7.7 fusion.114
  400.8 2.7 convolution_add_fusion.8
  404.0 8.6 %select_exponential_fusion.5 = f32[16,64,64,32]{2,3,1,0:T(8,128)} fusion(f32[16,64,32]{1,2,0:T(8,128)S(1)} %copy.175, f32[16,64,32]{2,1,0:T(8,128)S(1)} %copy.176, pred[64,64]{1,0:T(8,128)(4,1)S(1)} %iota_compare_fusion.5), kind=kLoop, calls=%fused_computation.34.clone.1 | loop fusion | flops 4194304 | bytes 8654848 | tf_op jit(solution)/shard_map/while/body/eval_jaxpr/exp | solution.py:54
  412.6 18.4 %copy.177 = f32[16,64,64,32]{1,2,3,0:T(8,128)} copy(f32[16,64,64,32]{2,3,1,0:T(8,128)} %select_exponential_fusion.5) | data formatting | bytes 16777216 | tf_op jit(solution)/shard_map/while
  432.6 7.7 fusion.114
  446.0 4.5 convolution_convert_fusion.1
  452.7 4.1 collective-permute-start.1
  456.9 37.0 %collective-permute-done = bf16[256,1536]{1,0:T(8,128)(2,1)S(1)} collective-permute-done((bf16[256,1536]{1,0:T(8,128)(2,1)S(1)}, bf16[256,1536]{1,0:T(8,128)(2,1)S(1)}, u32[]{:S(2)}, u32[]{:S(2)}) %collective-permute-start) | collective-permute-done | bytes 786464 | tf_op jit(solution)/shard_map/ppermute | solution.py:20
  493.8 2.5 collective-permute-start.2
  498.5 29.0 %collective-permute-done.2 = bf16[256,1536]{1,0:T(8,128)(2,1)} collective-permute-done((bf16[256,1536]{1,0:T(8,128)(2,1)S(1)}, bf16[256,1536]{1,0:T(8,128)(2,1)}, u32[]{:S(2)}, u32[]{:S(2)}) %collective-permute-start.2) | collective-permute-done | bytes 786464 | tf_op jit(solution)/shard_map/ppermute | solution.py:20
  527.6 2.2 collective-permute-start.4
  529.7 3.2 broadcast_in_dim.47
  534.8 2.4 collective-permute-start.5
  537.2 2.1 constant_dynamic-update-slice_fusion.5
  539.3 41.6 %collective-permute-done.4 = bf16[256,1536]{1,0:T(8,128)(2,1)S(1)} collective-permute-done((bf16[256,1536]{1,0:T(8,128)(2,1)}, bf16[256,1536]{1,0:T(8,128)(2,1)S(1)}, u32[]{:S(2)}, u32[]{:S(2)}) %collective-permute-start.4) | collective-permute-done | bytes 786464 | tf_op jit(solution)/shard_map/ppermute | solution.py:20
  580.8 2.4 collective-permute-start.6
  583.2 2.1 constant_dynamic-update-slice_fusion.4
  585.3 2.1 constant_dynamic-update-slice_fusion.3
  588.3 6.3 collective-permute-done.5
  595.6 16.8 %collective-permute-done.6 = bf16[256,1536]{1,0:T(8,128)(2,1)S(1)} collective-permute-done((bf16[256,1536]{1,0:T(8,128)(2,1)S(1)}, bf16[256,1536]{1,0:T(8,128)(2,1)S(1)}, u32[]{:S(2)}, u32[]{:S(2)}) %collective-permute-start.6) | collective-permute-done | bytes 786464 | tf_op jit(solution)/shard_map/ppermute | solution.py:20
  614.6 20.4 %all-gather.18.cloned.1.call-done = bf16[2048,1536]{1,0:T(8,128)(2,1)} async-done(((bf16[256,1536]{1,0:T(8,128)(2,1)}), bf16[2048,1536]{1,0:T(8,128)(2,1)}) %all-gather.18.cloned.1.call-update) | async-done | bytes 6291472 | tf_op jit(solution)/shard_map/all_gather | solution.py:139
  635.0 3.8 fusion.51
  638.9 95.9 %all-gather.20.cloned.1.call-done = bf16[2048,1536]{1,0:T(8,128)(2,1)} async-done(((bf16[256,1536]{1,0:T(8,128)(2,1)}), bf16[2048,1536]{1,0:T(8,128)(2,1)}) %all-gather.20.cloned.1.call-update) | async-done | bytes 6291472 | tf_op jit(solution)/shard_map/all_gather | solution.py:141
  734.7 8.6 %convolution_convert_fusion = bf16[128,2048]{1,0:T(8,128)(2,1)} fusion(bf16[2048,1536]{1,0:T(8,128)(2,1)} %all-gather.20.cloned.1.call-done, bf16[2048,1536]{1,0:T(8,128)(2,1)} %constant_dynamic-update-slice_fusion, f32[128,1536]{1,0:T(8,128)S(1)} %fusion.51, bf16[128,2048]{1,0:T(8,128)(2,1)S(1)} %get-tuple-element.214, f32[2048]{0:T(1024)S(1)} %copy-done.15, ...), kind=kOutput, calls=%fused_computation.60 | convolution fusion | flops 1613103104 | bytes 14426624 | tf_op jit(solution)/shard_map/dot_general | solution.py:152
  743.3 17.0 %all-reduce.5.cloned.1.call-done = bf16[128,2048]{1,0:T(8,128)(2,1)} async-done(((bf16[128,2048]{1,0:T(8,128)(2,1)}), bf16[128,2048]{1,0:T(8,128)(2,1)}) %all-reduce.5.cloned.1.call-update) | async-done | bytes 524304 | tf_op jit(solution)/shard_map/psum | solution.py:155
  760.3 2.0 fusion.45
  (163 shorter events, 73.1 us)
Async XLA Ops:
  6.5 104.5 %copy-start.4 = (bf16[128,2048]{1,0:T(8,128)(2,1)S(1)}, bf16[128,2048]{1,0:T(8,128)(2,1)}, u32[]{:S(2)}) copy-start(bf16[128,2048]{1,0:T(8,128)(2,1)} %param.18) | copy-start | bytes 1572868
  6.5 104.5 %copy-start.14 = (f32[2048]{0:T(1024)S(1)}, f32[2048]{0:T(1024)}, u32[]{:S(2)}) copy-start(f32[2048]{0:T(1024)} %param.19) | copy-start | bytes 24580
  6.5 54.8 %all-gather.8.cloned.1.call-start = ((), (), s32[]{:S(2)}) async-start(), calls=%async_computation | async-start | bytes 2359296 | tf_op jit(solution)/shard_map/all_gather | solution.py:110
  7.3 103.8 %all-gather.10.cloned.1.call-start = ((), (), s32[]{:S(2)}) async-start(), calls=%async_computation.1 | async-start | bytes 2359296 | tf_op jit(solution)/shard_map/all_gather | solution.py:108
  8.0 152.9 %all-gather.14.cloned.1.call-start = ((), (), s32[]{:S(2)}) async-start(), calls=%async_computation.3 | async-start | bytes 2359296 | tf_op jit(solution)/shard_map/all_gather | solution.py:107
  8.7 225.5 %all-gather.12.cloned.1.call-start = ((), (), s32[]{:S(2)}) async-start(), calls=%async_computation.2 | async-start | bytes 4718592 | tf_op jit(solution)/shard_map/all_gather | solution.py:109
  9.3 436.7 %all-gather.16.cloned.1.call-start = ((), (), s32[]{:S(2)}) async-start(), calls=%async_computation.4 | async-start | bytes 4718592 | tf_op jit(solution)/shard_map/all_gather | solution.py:111
  9.9 603.4 %all-reduce.3.cloned.1.call-start = ((), (), s32[]{:S(2)}) async-start(), calls=%async_computation.5 | async-start | bytes 1048576 | tf_op jit(solution)/shard_map/psum | solution.py:146
  12.0 152.2 %copy-start.13 = (f32[128,16]{0,1:T(8,128)S(1)}, f32[128,16]{0,1:T(8,128)}, u32[]{:S(2)}) copy-start(f32[128,16]{0,1:T(8,128)} %param.25) | copy-start | bytes 24580
  240.8 2.1 copy-start.2
  281.7 8.1 %copy-start.1 = (f32[2,16,64,64]{3,2,1,0:T(8,128)S(1)}, f32[2,16,64,64]{3,2,1,0:T(8,128)}, u32[]{:S(2)}) copy-start(f32[2,16,64,64]{3,2,1,0:T(8,128)} %get-tuple-element.362) | copy-start | bytes 1572868 | tf_op jit(solution)/shard_map/while
  281.7 8.1 %copy-start.8 = (f32[2,16,64,64]{3,2,1,0:T(8,128)S(1)}, f32[2,16,64,64]{3,2,1,0:T(8,128)}, u32[]{:S(2)}) copy-start(f32[2,16,64,64]{3,2,1,0:T(8,128)} %get-tuple-element.350) | copy-start | bytes 1572868 | tf_op jit(solution)/shard_map/while
  281.7 10.1 %copy-start.3 = (f32[2,16,64,32]{2,0,3,1:T(2,128)S(1)}, f32[2,16,64,32]{2,0,3,1:T(2,128)}, u32[]{:S(2)}) copy-start(f32[2,16,64,32]{2,0,3,1:T(2,128)} %copy-done.2) | copy-start | bytes 786436 | tf_op jit(solution)/shard_map/while
  290.8 1.0 copy-start.9
  291.8 2.1 copy-start.2
  332.5 8.0 %copy-start.1 = (f32[2,16,64,64]{3,2,1,0:T(8,128)S(1)}, f32[2,16,64,64]{3,2,1,0:T(8,128)}, u32[]{:S(2)}) copy-start(f32[2,16,64,64]{3,2,1,0:T(8,128)} %get-tuple-element.362) | copy-start | bytes 1572868 | tf_op jit(solution)/shard_map/while
  332.5 8.0 %copy-start.8 = (f32[2,16,64,64]{3,2,1,0:T(8,128)S(1)}, f32[2,16,64,64]{3,2,1,0:T(8,128)}, u32[]{:S(2)}) copy-start(f32[2,16,64,64]{3,2,1,0:T(8,128)} %get-tuple-element.350) | copy-start | bytes 1572868 | tf_op jit(solution)/shard_map/while
  332.5 10.0 %copy-start.3 = (f32[2,16,64,32]{2,0,3,1:T(2,128)S(1)}, f32[2,16,64,32]{2,0,3,1:T(2,128)}, u32[]{:S(2)}) copy-start(f32[2,16,64,32]{2,0,3,1:T(2,128)} %copy-done.2) | copy-start | bytes 786436 | tf_op jit(solution)/shard_map/while
  341.6 1.0 copy-start.9
  342.6 7.1 copy-start
  385.3 7.7 %copy-start.6 = (f32[2,16,64,64]{3,2,1,0:T(8,128)S(1)}, f32[2,16,64,64]{3,2,1,0:T(8,128)}, u32[]{:S(2)}) copy-start(f32[2,16,64,64]{3,2,1,0:T(8,128)} %get-tuple-element.377) | copy-start | bytes 1572868 | tf_op jit(solution)/shard_map/while
  394.0 1.0 copy-start.7
  432.5 7.7 %copy-start.6 = (f32[2,16,64,64]{3,2,1,0:T(8,128)S(1)}, f32[2,16,64,64]{3,2,1,0:T(8,128)}, u32[]{:S(2)}) copy-start(f32[2,16,64,64]{3,2,1,0:T(8,128)} %get-tuple-element.377) | copy-start | bytes 1572868 | tf_op jit(solution)/shard_map/while
  441.3 1.0 copy-start.7
  442.3 3.5 copy-start.16
  443.9 8.2 %copy-start.10 = (bf16[256,1536]{1,0:T(8,128)(2,1)S(1)}, bf16[256,1536]{1,0:T(8,128)(2,1)}, u32[]{:S(2)}) copy-start(bf16[256,1536]{1,0:T(8,128)(2,1)} %param.30) | copy-start | bytes 2359300
  450.5 184.5 %all-gather.18.cloned.1.call-start = ((), (), s32[]{:S(2)}) async-start(), calls=%async_computation.6 | async-start | bytes 7077888 | tf_op jit(solution)/shard_map/all_gather | solution.py:139
  451.3 283.5 %all-gather.20.cloned.1.call-start = ((), (), s32[]{:S(2)}) async-start(), calls=%async_computation.7 | async-start | bytes 7077888 | tf_op jit(solution)/shard_map/all_gather | solution.py:141
  452.0 308.2 %all-reduce.5.cloned.1.call-start = ((), (), s32[]{:S(2)}) async-start(), calls=%async_computation.8 | async-start | bytes 1048576 | tf_op jit(solution)/shard_map/psum | solution.py:155
  452.1 41.7 %collective-permute-start = (bf16[256,1536]{1,0:T(8,128)(2,1)S(1)}, bf16[256,1536]{1,0:T(8,128)(2,1)S(1)}, u32[]{:S(2)}, u32[]{:S(2)}) collective-permute-start(bf16[256,1536]{1,0:T(8,128)(2,1)S(1)} %copy-done.10), channel_id=1, source_target_pairs={{0,2},{2,4},{4,6},{6,8},{8,10},{10,12},{12,14},{14,0},{1,3},{3,5},... | collective-permute-start | bytes 2359304 | tf_op jit(solution)/shard_map/ppermute | solution.py:20
  452.7 45.2 %collective-permute-start.1 = (bf16[256,1536]{1,0:T(8,128)(2,1)S(1)}, bf16[256,1536]{1,0:T(8,128)(2,1)}, u32[]{:S(2)}, u32[]{:S(2)}) collective-permute-start(bf16[256,1536]{1,0:T(8,128)(2,1)S(1)} %copy-done.10), channel_id=1, source_target_pairs={{0,14},{2,0},{4,2},{6,4},{8,6},{10,8},{12,10},{14,12},{1,15},{3,1}... | collective-permute-start | bytes 2359304 | tf_op jit(solution)/shard_map/ppermute | solution.py:23
  493.8 4.7 copy-start.11
  493.8 33.7 %collective-permute-start.2 = (bf16[256,1536]{1,0:T(8,128)(2,1)S(1)}, bf16[256,1536]{1,0:T(8,128)(2,1)}, u32[]{:S(2)}, u32[]{:S(2)}) collective-permute-start(bf16[256,1536]{1,0:T(8,128)(2,1)S(1)} %collective-permute-done), channel_id=1, source_target_pairs={{0,2},{2,4},{4,6},{6,8},{8,10},{10,12},{12,14},{14,0},{1,3},{3,5},... | collective-permute-start | bytes 2359304 | tf_op jit(solution)/shard_map/ppermute | solution.py:20
  497.9 36.9 %collective-permute-start.3 = (bf16[256,1536]{1,0:T(8,128)(2,1)}, bf16[256,1536]{1,0:T(8,128)(2,1)}, u32[]{:S(2)}, u32[]{:S(2)}) collective-permute-start(bf16[256,1536]{1,0:T(8,128)(2,1)} %collective-permute-done.1), channel_id=1, source_target_pairs={{0,14},{2,0},{4,2},{6,4},{8,6},{10,8},{12,10},{14,12},{1,15},{3,1}... | collective-permute-start | bytes 2359304 | tf_op jit(solution)/shard_map/ppermute | solution.py:23
  527.6 53.3 %collective-permute-start.4 = (bf16[256,1536]{1,0:T(8,128)(2,1)}, bf16[256,1536]{1,0:T(8,128)(2,1)S(1)}, u32[]{:S(2)}, u32[]{:S(2)}) collective-permute-start(bf16[256,1536]{1,0:T(8,128)(2,1)} %collective-permute-done.2), channel_id=1, source_target_pairs={{0,2},{2,4},{4,6},{6,8},{8,10},{10,12},{12,14},{14,0},{1,3},{3,5},... | collective-permute-start | bytes 2359304 | tf_op jit(solution)/shard_map/ppermute | solution.py:20
  529.7 4.1 copy-start.12
  532.9 80.4 %copy-start.5 = (bf16[128,2048]{1,0:T(8,128)(2,1)S(1)}, bf16[128,2048]{1,0:T(8,128)(2,1)}, u32[]{:S(2)}) copy-start(bf16[128,2048]{1,0:T(8,128)(2,1)} %param.18) | copy-start | bytes 1572868
  533.9 101.2 %copy-start.15 = (f32[2048]{0:T(1024)S(1)}, f32[2048]{0:T(1024)}, u32[]{:S(2)}) copy-start(f32[2048]{0:T(1024)} %param.28) | copy-start | bytes 24580
  534.8 59.8 %collective-permute-start.5 = (bf16[256,1536]{1,0:T(8,128)(2,1)}, bf16[256,1536]{1,0:T(8,128)(2,1)S(1)}, u32[]{:S(2)}, u32[]{:S(2)}) collective-permute-start(bf16[256,1536]{1,0:T(8,128)(2,1)} %collective-permute-done.3), channel_id=1, source_target_pairs={{0,14},{2,0},{4,2},{6,4},{8,6},{10,8},{12,10},{14,12},{1,15},{3,1}... | collective-permute-start | bytes 2359304 | tf_op jit(solution)/shard_map/ppermute | solution.py:23
  580.8 31.5 %collective-permute-start.6 = (bf16[256,1536]{1,0:T(8,128)(2,1)S(1)}, bf16[256,1536]{1,0:T(8,128)(2,1)S(1)}, u32[]{:S(2)}, u32[]{:S(2)}) collective-permute-start(bf16[256,1536]{1,0:T(8,128)(2,1)S(1)} %collective-permute-done.4), channel_id=1, source_target_pairs={{0,2},{2,4},{4,6},{6,8},{8,10},{10,12},{12,14},{14,0},{1,3},{3,5},... | collective-permute-start | bytes 2359304 | tf_op jit(solution)/shard_map/ppermute | solution.py:20
Sparse Core Ops, SparseCore 0:
  9.5 51.7 all-gather.7
  63.4 47.6 all-gather.9
  113.2 47.6 all-gather.13
  162.8 71.3 all-gather.11
  236.2 71.3 all-gather.15
  450.7 17.1 all-reduce.2
  470.0 164.9 all-gather.17
  637.2 97.4 all-gather.19
  743.4 16.7 all-reduce.4
